TPU v7x, 32 devices: a whole 2x2x4 slice. The times are simulated.
32 devices in a mesh: st: 16 (over z, y, x), tp: 2 (over core).
Axes of the slice: x: 2, y: 2, z: 4, core: 2. Of those that a mesh axis runs over, the one named last changes fastest.
Arguments:
- tokens: bfloat16 [4096, 2048], P('st'), may hold values from -6 to 6
- store: bfloat16 [64, 64, 2048], P('st'), may hold values from -6 to 6
- passage_ids: int32 [64, 4], P('st'), may hold values from 0 to 63, as said below
- w_query: bfloat16 [2048, 2048], P(None, 'tp'), may hold values from -0.125 to 0.125
- w_key: bfloat16 [2048, 512], P(None, 'tp'), may hold values from -0.125 to 0.125
- w_value: bfloat16 [2048, 512], P(None, 'tp'), may hold values from -0.125 to 0.125
- w_ret_query: bfloat16 [2048, 1024], P(None, 'tp'), may hold values from -0.125 to 0.125
- w_ret_key: bfloat16 [2048, 1024], P(None, 'tp'), may hold values from -0.125 to 0.125
- w_ret_value: bfloat16 [2048, 2048], P(None, 'tp'), may hold values from -0.125 to 0.125
- ret_rate: float32 [8], P('tp'), may hold values from 0.003 to 0.03
- ret_gain: float32 [2048], P('tp'), may hold values from 0.1 to 1.9
- gate_logit: float32 [2048], P('tp'), may hold values from -2 to 2
- out_grad: bfloat16 [4096, 2048], P('st', 'tp'), may hold values from -6 to 6
Outputs:
- grad_tokens: bfloat16 [4096, 2048], P(('st', 'tp'))
- grad_store: bfloat16 [64, 64, 2048], P(('st', 'tp'))
- grad_key_weight: float32 [2048, 512], P(None, 'tp')
Inputs may be any that keep to these rules, and one draw needn't show every extreme that they name: `passage_ids`: passage p lies on index p // 4 of st. The rows of one device name exactly 1 passage of every owner, so the 4 passages of a block differ.
All inputs are finite; a program needn't handle non-finite values.
Results may differ from a plain program's by a relative error of at most 0.012.
Values may be sent and summed in bfloat16 or wider, within the bound.
A program may use at most 192 MiB of HBM per device.

v0:
```python
import jax
import jax.numpy as jnp
from jax import lax
from jax.sharding import PartitionSpec as P

HEAD = 256
BLK = 64
KP = 4
MOST = 1
EPSILON = 1.0


def retention_grads(query_rows, key_rows, value_rows, rates, gains, cotangent):
    length = query_rows.shape[0]
    heads = rates.shape[0]
    queries = query_rows.reshape(length, heads, -1)
    keyset = key_rows.reshape(length, heads, -1)
    values = value_rows.reshape(length, heads, -1)
    positions = jnp.arange(length, dtype=jnp.float32)
    distance = positions[:, None] - positions[None, :]
    damping = jnp.where(
        distance >= 0.0, jnp.exp(-rates[:, None, None] * jnp.maximum(distance, 0.0)), 0.0
    ) * queries.shape[-1] ** (-0.5)
    raw = jnp.einsum("thd,shd->hts", queries, keyset, preferred_element_type=jnp.float32)
    weights = (raw * damping).astype(jnp.bfloat16)
    mixed = jnp.einsum("hts,she->the", weights, values, preferred_element_type=jnp.float32)
    inverse = lax.rsqrt(jnp.mean(mixed * mixed, axis=-1, keepdims=True) + EPSILON)
    scaled = cotangent.astype(jnp.float32).reshape(length, heads, -1) * gains.reshape(heads, -1)
    inner = jnp.mean(scaled * mixed, axis=-1, keepdims=True)
    grad_mixed = (inverse * scaled - inverse * inverse * inverse * mixed * inner).astype(
        jnp.bfloat16
    )
    grad_weights = (
        jnp.einsum("the,she->hts", grad_mixed, values, preferred_element_type=jnp.float32) * damping
    ).astype(jnp.bfloat16)
    grad_first = (
        jnp.einsum("hts,shd->thd", grad_weights, keyset, preferred_element_type=jnp.float32)
        .astype(jnp.bfloat16)
        .reshape(length, -1)
    )
    grad_second = (
        jnp.einsum("hts,thd->shd", grad_weights, queries, preferred_element_type=jnp.float32)
        .astype(jnp.bfloat16)
        .reshape(length, -1)
    )
    grad_third = (
        jnp.einsum("hts,the->she", weights, grad_mixed, preferred_element_type=jnp.float32)
        .astype(jnp.bfloat16)
        .reshape(length, -1)
    )
    return (grad_first, grad_second, grad_third)


def against_rows(left, weight):
    return lax.dot_general(
        left, weight, (((1,), (1,)), ((), ())), preferred_element_type=jnp.float32
    )


def across_rows(left, right):
    return lax.dot_general(
        left, right, (((0,), (0,)), ((), ())), preferred_element_type=jnp.float32
    )


def per_device(
    tokens,
    store,
    passage_ids,
    w_query,
    w_key,
    w_value,
    w_ret_query,
    w_ret_key,
    w_ret_value,
    ret_rate,
    ret_gain,
    gate_logit,
    out_grad,
):
    owners = lax.axis_size("st")
    pass_dev, plen, width = store.shape
    length = tokens.shape[0]
    kv_width = w_key.shape[1]
    kv_local = kv_width // HEAD
    group = w_query.shape[1] // HEAD // kv_local
    blocks = length // BLK
    slot_ids = passage_ids.reshape(-1)
    slot_count = slot_ids.shape[0]
    slot_owner = slot_ids // pass_dev
    slot_local = slot_ids % pass_dev
    order = jnp.arange(slot_count, dtype=jnp.int32)
    same_owner = slot_owner[:, None] == slot_owner[None, :]
    rank = jnp.sum(same_owner & (order[None, :] < order[:, None]), axis=1)
    position = slot_owner * MOST + rank
    cells = owners * MOST
    placed = jnp.arange(cells, dtype=jnp.int32)[:, None] == position[None, :]
    request = (jnp.sum(jnp.where(placed, slot_local[None, :] + 1, 0), axis=1) - 1).reshape(
        owners, MOST
    )
    incoming = lax.all_to_all(request, "st", split_axis=0, concat_axis=0, tiled=True)
    wanted = incoming.reshape(-1)
    valid = wanted >= 0
    safe = jnp.maximum(wanted, 0)
    placed_bf = placed.astype(jnp.bfloat16)
    store_rows = store.reshape(-1, width)
    nothing = jnp.zeros((), jnp.bfloat16)
    own_kv = jnp.concatenate(
        [
            jnp.dot(store_rows, w_key, preferred_element_type=jnp.float32).astype(jnp.bfloat16),
            jnp.dot(store_rows, w_value, preferred_element_type=jnp.float32).astype(jnp.bfloat16),
        ],
        axis=1,
    ).reshape(pass_dev, plen, 2 * kv_width)
    reply = jnp.where(valid[:, None, None], own_kv[safe], nothing).reshape(
        owners, MOST, plen, 2 * kv_width
    )
    arrived = lax.all_to_all(reply, "st", split_axis=0, concat_axis=0, tiled=True)
    slot_kv = (
        across_rows(placed_bf, arrived.reshape(cells, -1))
        .astype(jnp.bfloat16)
        .reshape(slot_count, plen, 2 * kv_width)
    )
    factor = HEAD ** (-0.5)
    gate = jax.nn.sigmoid(gate_logit)
    query_bf = jnp.dot(tokens, w_query, preferred_element_type=jnp.float32).astype(jnp.bfloat16)
    queries = query_bf.reshape(blocks, BLK, kv_local, group, HEAD)
    keys = slot_kv[:, :, :kv_width].reshape(blocks, KP * plen, kv_local, HEAD)
    values = slot_kv[:, :, kv_width:].reshape(blocks, KP * plen, kv_local, HEAD)
    scores = (
        jnp.einsum("btkgd,bskd->bkgts", queries, keys, preferred_element_type=jnp.float32) * factor
    )
    expo = jnp.exp(scores)
    probs = expo / jnp.sum(expo, axis=-1, keepdims=True)
    probs_bf = probs.astype(jnp.bfloat16)
    attn = jnp.einsum("bkgts,bskd->btkgd", probs_bf, values, preferred_element_type=jnp.float32)
    grad_attn = out_grad.astype(jnp.float32).reshape(
        blocks, BLK, kv_local, group, HEAD
    ) * gate.reshape(kv_local, group, HEAD)
    grad_attn_bf = grad_attn.astype(jnp.bfloat16)
    grad_probs = jnp.einsum(
        "btkgd,bskd->bkgts", grad_attn_bf, values, preferred_element_type=jnp.float32
    )
    delta = jnp.moveaxis(jnp.sum(grad_attn * attn, axis=-1), 1, 3)
    grad_scores = (probs * (grad_probs - delta[..., None]) * factor).astype(jnp.bfloat16)
    grad_query = (
        jnp.einsum("bkgts,bskd->btkgd", grad_scores, keys, preferred_element_type=jnp.float32)
        .astype(jnp.bfloat16)
        .reshape(length, -1)
    )
    grad_keys = (
        jnp.einsum("bkgts,btkgd->bskd", grad_scores, queries, preferred_element_type=jnp.float32)
        .astype(jnp.bfloat16)
        .reshape(slot_count, plen, kv_width)
    )
    grad_values = (
        jnp.einsum("bkgts,btkgd->bskd", probs_bf, grad_attn_bf, preferred_element_type=jnp.float32)
        .astype(jnp.bfloat16)
        .reshape(slot_count, plen, kv_width)
    )
    slot_grad = jnp.concatenate([grad_keys, grad_values], axis=2)
    outgoing = (
        jnp.dot(placed_bf, slot_grad.reshape(slot_count, -1), preferred_element_type=jnp.float32)
        .astype(jnp.bfloat16)
        .reshape(owners, MOST, plen, 2 * kv_width)
    )
    returned = lax.all_to_all(outgoing, "st", split_axis=0, concat_axis=0, tiled=True)
    matched = (jnp.arange(pass_dev, dtype=jnp.int32)[:, None] == wanted[None, :]).astype(
        jnp.bfloat16
    )
    passage_grad = jnp.dot(
        matched, returned.reshape(cells, -1), preferred_element_type=jnp.float32
    ).reshape(pass_dev * plen, 2 * kv_width)
    key_grad = passage_grad[:, :kv_width]
    upper = key_grad.astype(jnp.bfloat16)
    lower = (key_grad - upper.astype(jnp.float32)).astype(jnp.bfloat16)
    key_term = across_rows(store_rows, upper) + across_rows(store_rows, lower)
    grad_key_weight = lax.psum(key_term, "st")
    passage_bf = passage_grad.astype(jnp.bfloat16)
    grad_store = lax.psum_scatter(
        (
            against_rows(passage_bf[:, :kv_width], w_key)
            + against_rows(passage_bf[:, kv_width:], w_value)
        ).astype(jnp.bfloat16),
        "tp",
        scatter_dimension=0,
        tiled=True,
    ).astype(jnp.float32)
    grad_store = grad_store.astype(jnp.bfloat16).reshape(-1, plen, width)
    ret_query = jnp.dot(tokens, w_ret_query, preferred_element_type=jnp.float32).astype(
        jnp.bfloat16
    )
    ret_key = jnp.dot(tokens, w_ret_key, preferred_element_type=jnp.float32).astype(jnp.bfloat16)
    ret_value = jnp.dot(tokens, w_ret_value, preferred_element_type=jnp.float32).astype(
        jnp.bfloat16
    )
    grad_rq, grad_rk, grad_rv = retention_grads(
        ret_query, ret_key, ret_value, ret_rate, ret_gain, out_grad
    )
    total = against_rows(grad_query, w_query)
    total = total + against_rows(grad_rq, w_ret_query)
    total = total + against_rows(grad_rk, w_ret_key)
    grad_tokens = lax.psum_scatter(
        (total + against_rows(grad_rv, w_ret_value)).astype(jnp.bfloat16),
        "tp",
        scatter_dimension=0,
        tiled=True,
    )
    return (grad_tokens, grad_store, grad_key_weight)


def solution(mesh):
    return jax.shard_map(
        per_device,
        mesh=mesh,
        in_specs=(
            P("st", None),
            P("st", None, None),
            P("st", None),
            P(None, "tp"),
            P(None, "tp"),
            P(None, "tp"),
            P(None, "tp"),
            P(None, "tp"),
            P(None, "tp"),
            P("tp"),
            P("tp"),
            P("tp"),
            P("st", "tp"),
        ),
        out_specs=(P(("st", "tp"), None), P(("st", "tp"), None, None), P(None, "tp")),
        check_vma=False,
    )
```

profile of v0, /device:TPU:0, one launch (start us, length us, event | category | flops | bytes accessed | tf_op | source)
XLA Modules:
  0.0 243.0 jit_solution(17686899952723807470)
XLA Ops:
  10.0 8.3 %all-to-all-start = ((s32[16,1,1]{2,1,0:T(1,128)}), s32[16,1,1]{2,1,0:T(1,128)S(1)}, u32[]{:S(2)}, u32[]{:S(2)}) async-start(s32[16,1,1]{2,1,0:T(1,128)} %copy.79), calls=%async_computation | async-start | bytes 16384 | tf_op jit(solution)/shard_map/all_to_all | solution.py:101
  18.3 2.1 convolution_convert_fusion.10
  22.9 2.7 %all-to-all-done = s32[16,1,1]{2,1,0:T(1,128)S(1)} async-done(((s32[16,1,1]{2,1,0:T(1,128)}), s32[16,1,1]{2,1,0:T(1,128)S(1)}, u32[]{:S(2)}, u32[]{:S(2)}) %all-to-all-start) | async-done | bytes 96 | tf_op jit(solution)/shard_map/all_to_all | solution.py:101
  28.2 2.4 fusion.18
  30.6 4.3 %all-to-all-start.1 = ((bf16[16,1,64,512]{3,2,1,0:T(8,128)(2,1)}), bf16[16,1,64,512]{3,2,1,0:T(8,128)(2,1)}, u32[]{:S(2)}, u32[]{:S(2)}) async-start(bf16[16,1,64,512]{3,2,1,0:T(8,128)(2,1)} %fusion.18), calls=%async_computation.1 | async-start | bytes 2097152 | tf_op jit(solution)/shard_map/all_to_all | solution.py:118
  34.9 2.2 copy.89
  37.2 2.5 %reshape.312 = f32[4,64,4,256]{3,2,1,0:T(4,128)} reshape(bf16[256,1024]{1,0:T(8,128)(2,1)} %param.25) | data formatting | bytes 1572864 | tf_op jit(solution)/shard_map/reshape | solution.py:137
  39.7 2.5 %reshape.313 = f32[4,64,1,4,256]{4,3,1,0,2:T(4,128)} reshape(bf16[256,1024]{1,0:T(8,128)(2,1)} %param.25) | data formatting | bytes 1572864 | tf_op jit(solution)/shard_map/reshape | solution.py:137
  42.2 1.9 convolution_convert_fusion.8
  45.0 3.3 %convolution_convert_fusion.9 = bf16[256,512]{1,0:T(8,128)(2,1)} fusion(bf16[256,2048]{1,0:T(8,128)(2,1)} %param.13, bf16[2048,512]{1,0:T(8,128)(2,1)} %param.20), kind=kOutput, calls=%fused_computation.40 | convolution fusion | flops 537001984 | bytes 3407872 | tf_op jit(solution)/shard_map/dot_general | solution.py:193
  49.4 4.6 %convolution_convert_fusion.5 = bf16[256,1024]{1,0:T(8,128)(2,1)} fusion(bf16[256,2048]{1,0:T(8,128)(2,1)} %param.13, bf16[2048,1024]{1,0:T(8,128)(2,1)} %param.16), kind=kOutput, calls=%fused_computation.33 | convolution fusion | flops 1074003968 | bytes 5767168 | tf_op jit(solution)/shard_map/dot_general | solution.py:126
  54.0 2.2 reshape.310
  58.7 1.8 copy.105
  68.2 6.0 %all-to-all-start.2 = ((bf16[16,1,64,512]{3,2,1,0:T(8,128)(2,1)}), bf16[16,1,64,512]{3,2,1,0:T(8,128)(2,1)}, u32[]{:S(2)}, u32[]{:S(2)}) async-start(bf16[16,1,64,512]{3,2,1,0:T(8,128)(2,1)} %bitcast.183), calls=%async_computation.3 | async-start | bytes 2097152 | tf_op jit(solution)/shard_map/all_to_all | solution.py:167
  75.9 4.0 %convolution_convert_fusion.4 = bf16[256,1024]{1,0:T(8,128)(2,1)S(1)} fusion(bf16[256,2048]{1,0:T(8,128)(2,1)} %param.13, bf16[2048,1024]{1,0:T(8,128)(2,1)} %param.21), kind=kOutput, calls=%fused_computation.32 | convolution fusion | flops 1074003968 | bytes 5767168 | tf_op jit(solution)/shard_map/dot_general | solution.py:194
  83.6 13.5 %all-to-all-done.2 = bf16[16,1,64,512]{3,2,1,0:T(8,128)(2,1)} async-done(((bf16[16,1,64,512]{3,2,1,0:T(8,128)(2,1)}), bf16[16,1,64,512]{3,2,1,0:T(8,128)(2,1)}, u32[]{:S(2)}, u32[]{:S(2)}) %all-to-all-start.2) | async-done | bytes 1048608 | tf_op jit(solution)/shard_map/all_to_all | solution.py:167
  97.2 1.8 copy.110
  100.1 2.2 reshape.329
  103.8 1.8 fusion.1
  107.4 3.7 %fusion.49 = f32[256,2048]{1,0:T(8,128)S(1)} fusion(bf16[256,1024]{0,1:T(8,128)(2,1)S(1)} %bitcast.195, bf16[2048,1024]{1,0:T(8,128)(2,1)} %param.21), kind=kOutput, calls=%fused_computation.101 | convolution fusion | flops 1073741824 | bytes 6815744 | tf_op jit(solution)/shard_map/dot_general | solution.py:55
  114.8 1.7 fusion.2
  116.7 1.8 fusion.34
  120.0 112.7 %all-reduce.2.cloned.1.call-done = f32[2048,256]{0,1:T(8,128)} async-done(((f32[2048,256]{0,1:T(8,128)}), f32[2048,256]{0,1:T(8,128)}) %all-reduce.2.cloned.1.call-update) | async-done | bytes 2097168 | tf_op jit(solution)/shard_map/psum | solution.py:178
  232.7 2.9 %copy.96 = f32[2048,256]{1,0:T(8,128)} copy(f32[2048,256]{0,1:T(8,128)} %all-reduce.2.cloned.1.call-done) | data formatting | bytes 4194304
  (114 shorter events, 34.1 us)
Async XLA Ops:
  8.0 34.2 %copy-start = (bf16[2048,512]{1,0:T(8,128)(2,1)S(1)}, bf16[2048,512]{1,0:T(8,128)(2,1)}, u32[]{:S(2)}) copy-start(bf16[2048,512]{1,0:T(8,128)(2,1)} %param.19) | copy-start | bytes 6291460
  8.0 12.5 %copy-start.1 = (bf16[4,64,2048]{2,1,0:T(8,128)(2,1)S(1)}, bf16[4,64,2048]{2,1,0:T(8,128)(2,1)}, u32[]{:S(2)}) copy-start(bf16[4,64,2048]{2,1,0:T(8,128)(2,1)} %param.14) | copy-start | bytes 3145732
  10.0 15.6 %all-to-all-start = ((s32[16,1,1]{2,1,0:T(1,128)}), s32[16,1,1]{2,1,0:T(1,128)S(1)}, u32[]{:S(2)}, u32[]{:S(2)}) async-start(s32[16,1,1]{2,1,0:T(1,128)} %copy.79), calls=%async_computation | async-start | bytes 16384 | tf_op jit(solution)/shard_map/all_to_all | solution.py:101
  18.3 2.2 copy-start.8
  30.6 28.1 %all-to-all-start.1 = ((bf16[16,1,64,512]{3,2,1,0:T(8,128)(2,1)}), bf16[16,1,64,512]{3,2,1,0:T(8,128)(2,1)}, u32[]{:S(2)}, u32[]{:S(2)}) async-start(bf16[16,1,64,512]{3,2,1,0:T(8,128)(2,1)} %fusion.18), calls=%async_computation.1 | async-start | bytes 2097152 | tf_op jit(solution)/shard_map/all_to_all | solution.py:118
  34.9 7.3 %copy-start.26 = (f32[4]{0:T(128)S(1)}, f32[4]{0:T(128)}, u32[]{:S(2)}) copy-start(f32[4]{0:T(128)} %param.22) | copy-start | bytes 52
  34.9 7.2 %copy-start.23 = (f32[1024]{0:T(1024)S(1)}, f32[1024]{0:T(1024)}, u32[]{:S(2)}) copy-start(f32[1024]{0:T(1024)} %param.23) | copy-start | bytes 12292
  34.9 7.2 %copy-start.24 = (f32[1024]{0:T(1024)S(1)}, f32[1024]{0:T(1024)}, u32[]{:S(2)}) copy-start(f32[1024]{0:T(1024)} %param.24) | copy-start | bytes 12292
  68.2 29.0 %all-to-all-start.2 = ((bf16[16,1,64,512]{3,2,1,0:T(8,128)(2,1)}), bf16[16,1,64,512]{3,2,1,0:T(8,128)(2,1)}, u32[]{:S(2)}, u32[]{:S(2)}) async-start(bf16[16,1,64,512]{3,2,1,0:T(8,128)(2,1)} %bitcast.183), calls=%async_computation.3 | async-start | bytes 2097152 | tf_op jit(solution)/shard_map/all_to_all | solution.py:167
  74.1 158.6 %all-reduce.2.cloned.1.call-start = ((), (), s32[]{:S(2)}) async-start(), calls=%async_computation.7 | async-start | bytes 4194304 | tf_op jit(solution)/shard_map/psum | solution.py:178
  75.9 4.0 %copy-start.14 = (bf16[4,256,256]{2,1,0:T(8,128)(2,1)}, bf16[4,256,256]{2,1,0:T(8,128)(2,1)S(1)}, u32[]{:S(2)}) copy-start(bf16[4,256,256]{2,1,0:T(8,128)(2,1)S(1)} %fusion.10) | copy-start | bytes 1572868
  75.9 4.0 %copy-start.2 = (f32[256,1024]{0,1:T(8,128)S(1)}, f32[256,1024]{0,1:T(8,128)}, u32[]{:S(2)}) copy-start(f32[256,1024]{0,1:T(8,128)} %copy.89) | copy-start | bytes 3145732
  102.3 1.5 copy-start.6
  105.5 1.5 copy-start.13
  105.5 1.5 copy-start.15
  105.6 130.0 %reduce-scatter.3.cloned.1.call-start = ((), (), s32[]{:S(2)}) async-start(), calls=%async_computation.5 | async-start | bytes 1572864 | tf_op jit(solution)/shard_map/reduce_scatter | solution.py:203
  107.4 3.7 %copy-start.5 = (bf16[16,64,256]{2,1,0:T(8,128)(2,1)S(1)}, bf16[16,64,256]{2,1,0:T(8,128)(2,1)}, u32[]{:S(2)}) copy-start(bf16[16,64,256]{2,1,0:T(8,128)(2,1)} %copy-done.4) | copy-start | bytes 1572868
  107.4 3.7 %copy-start.11 = (bf16[4,4,64,256]{3,2,1,0:T(8,128)(2,1)S(1)}, bf16[4,4,64,256]{3,2,1,0:T(8,128)(2,1)}, u32[]{:S(2)}) copy-start(bf16[4,4,64,256]{3,2,1,0:T(8,128)(2,1)} %copy-done.10) | copy-start | bytes 1572868
  107.4 4.5 %copy-start.25 = (bf16[2048,1024]{1,0:T(8,128)(2,1)S(1)}, bf16[2048,1024]{1,0:T(8,128)(2,1)}, u32[]{:S(2)}) copy-start(bf16[2048,1024]{1,0:T(8,128)(2,1)} %param.16) | copy-start | bytes 12582916
  113.2 1.6 copy-start.17
  113.3 1.6 copy-start.21
  114.8 1.8 copy-start.7
  116.6 119.0 %reduce-scatter.5.cloned.1.call-start = ((), (), s32[]{:S(2)}) async-start(), calls=%async_computation.6 | async-start | bytes 1572864 | tf_op jit(solution)/shard_map/reduce_scatter | solution.py:180
  116.7 1.8 copy-start.9
  (9 other events, 9.6 us)
Sparse Core Ops, SparseCore 0:
  105.7 126.9 all-reduce.1
Sparse Core Ops, SparseCore 1:
  116.7 8.7 reduce-scatter.2
  128.1 9.5 reduce-scatter.4
where the time goes:
time: 244 us; the launch traced here: 243 us
  waiting for transfers between devices  131 us (54%)
  matrix products  40.1 us (16%)
  local copies, waits for them, and re-layouts  31.6 us (13%)
  starting transfers between devices  19 us (8%)
  between operations  16 us (7%)
  other arithmetic  5.71 us (2%)
    psum x1, waiting for transfers between devices, per_device(): grad_key_weight = lax.psum(key_term, 'st')  113 us
    all_to_all x1, waiting for transfers between devices, per_device(): lax.all_to_all(outgoing, 'st', split_axis=0, concat_axis=0, tiled=True)  13.5 us
    unnamed x61, local copies, waits for them, and re-layouts  13.2 us
    dot_general x6, matrix products, against_rows(): lax.dot_general(left, weight, (((1,), (1,)), ((), ())), preferred_element...  10.7 us
    all_to_all x1, starting transfers between devices, per_device(): lax.all_to_all(request, 'st', split_axis=0, concat_axis=0, tiled=True)  8.34 us
    all_to_all x1, starting transfers between devices, per_device(): lax.all_to_all(outgoing, 'st', split_axis=0, concat_axis=0, tiled=True)  5.96 us
    reshape x2, local copies, waits for them, and re-layouts, per_device(): out_grad.astype(jnp.float32).reshape(blocks, BLK, kv_local, group, HEAD)  4.98 us
  transfers between devices with their start and end apart: 6, of which 4 were waited for; matrix products, arithmetic and copies ran while one was open for 21% of the time, Pallas kernels for 0%

commit v1 on v0

--- a/solution.py
+++ b/solution.py
@@ -8,6 +8,15 @@
 KP = 4
 MOST = 1
 EPSILON = 1.0
+
+
+def sum_by_hops(value, mesh_axis):
+    size = lax.axis_size(mesh_axis)
+    total, stride = (value, 1)
+    while stride < size:
+        total = total + lax.ppermute(total, mesh_axis, [(i, i ^ stride) for i in range(size)])
+        stride = 2 * stride
+    return total
 
 
 def retention_grads(query_rows, key_rows, value_rows, rates, gains, cotangent):
@@ -175,7 +184,7 @@
     upper = key_grad.astype(jnp.bfloat16)
     lower = (key_grad - upper.astype(jnp.float32)).astype(jnp.bfloat16)
     key_term = across_rows(store_rows, upper) + across_rows(store_rows, lower)
-    grad_key_weight = lax.psum(key_term, "st")
+    grad_key_weight = sum_by_hops(key_term, "st")
     passage_bf = passage_grad.astype(jnp.bfloat16)
     grad_store = lax.psum_scatter(
         (

time: 244 us -> 356 us (1.46)
  waiting for transfers between devices: 131 us -> 230 us
  other arithmetic: 5.71 us -> 17 us
  starting transfers between devices: 19 us -> 29.3 us
  matrix products: 40.1 us -> 34.2 us
    ppermute x0 -> x4, waiting for transfers between devices: none -> 196 us  [sum_by_hops(): lax.ppermute(total, mesh_axis, [(i, i ^ stride) for i in range(size)])]
    psum x1 -> x0, waiting for transfers between devices: 113 us -> none  [per_device(): grad_key_weight = lax.psum(key_term, 'st')]
    add x0 -> x4, other arithmetic: none -> 12.1 us  [sum_by_hops(): total + lax.ppermute(total, mesh_axis, [(i, i ^ stride) for i in range(si...]
    ppermute x0 -> x4, starting transfers between devices: none -> 10.4 us  [sum_by_hops(): lax.ppermute(total, mesh_axis, [(i, i ^ stride) for i in range(size)])]
    all_to_all x1, waiting for transfers between devices: 1.66 us -> 12 us  [per_device(): lax.all_to_all(reply, 'st', split_axis=0, concat_axis=0, tiled=True)]
    all_to_all x1, waiting for transfers between devices: 13.5 us -> 20.2 us  [per_device(): lax.all_to_all(outgoing, 'st', split_axis=0, concat_axis=0, tiled=True)]
    unnamed x61 -> x53, local copies, waits for them, and re-layouts: 13.2 us -> 11.3 us
  transfers between devices with their start and end apart: 6 -> 9, of which waited for: 4 -> 7; matrix products, arithmetic and copies ran while one was open for 21% -> 14% of each run, Pallas kernels for 0% -> 0%
where the time goes in v1:
time: 356 us; the launch traced here: 355 us
  waiting for transfers between devices  230 us (65%)
  matrix products  34.2 us (10%)
  local copies, waits for them, and re-layouts  29.6 us (8%)
  starting transfers between devices  29.3 us (8%)
  other arithmetic  17 us (5%)
  between operations  14.6 us (4%)
    ppermute x4, waiting for transfers between devices, sum_by_hops(): lax.ppermute(total, mesh_axis, [(i, i ^ stride) for i in range(size)])  196 us
    all_to_all x1, waiting for transfers between devices, per_device(): lax.all_to_all(outgoing, 'st', split_axis=0, concat_axis=0, tiled=True)  20.2 us
    add x4, other arithmetic, sum_by_hops(): total + lax.ppermute(total, mesh_axis, [(i, i ^ stride) for i in range(si...  12.1 us
    all_to_all x1, waiting for transfers between devices, per_device(): lax.all_to_all(reply, 'st', split_axis=0, concat_axis=0, tiled=True)  12 us
    unnamed x53, local copies, waits for them, and re-layouts  11.3 us
    ppermute x4, starting transfers between devices, sum_by_hops(): lax.ppermute(total, mesh_axis, [(i, i ^ stride) for i in range(size)])  10.4 us
    all_to_all x1, starting transfers between devices, per_device(): lax.all_to_all(request, 'st', split_axis=0, concat_axis=0, tiled=True)  8.34 us
    dot_general x6, matrix products, against_rows(): lax.dot_general(left, weight, (((1,), (1,)), ((), ())), preferred_element...  8.27 us
  transfers between devices with their start and end apart: 9, of which 7 were waited for; matrix products, arithmetic and copies ran while one was open for 14% of the time, Pallas kernels for 0%

profile of v1, /device:TPU:0, one launch (start us, length us, event | category | flops | bytes accessed | tf_op | source)
XLA Modules:
  0.0 355.2 jit_solution(11450373126892977765)
XLA Ops:
  9.1 8.3 %all-to-all-start = ((s32[16,1,1]{2,1,0:T(1,128)}), s32[16,1,1]{2,1,0:T(1,128)S(1)}, u32[]{:S(2)}, u32[]{:S(2)}) async-start(s32[16,1,1]{2,1,0:T(1,128)} %copy.79), calls=%async_computation | async-start | bytes 16384 | tf_op jit(solution)/shard_map/all_to_all | solution.py:110
  22.0 2.7 all-to-all-done
  27.4 2.3 fusion.18
  29.7 4.4 %all-to-all-start.1 = ((bf16[16,1,64,512]{3,2,1,0:T(8,128)(2,1)}), bf16[16,1,64,512]{3,2,1,0:T(8,128)(2,1)}, u32[]{:S(2)}, u32[]{:S(2)}) async-start(bf16[16,1,64,512]{3,2,1,0:T(8,128)(2,1)} %fusion.18), calls=%async_computation.1 | async-start | bytes 2097152 | tf_op jit(solution)/shard_map/all_to_all | solution.py:127
  34.1 2.5 reshape.312
  36.6 2.5 reshape.313
  39.1 4.6 %convolution_convert_fusion.5 = bf16[256,1024]{1,0:T(8,128)(2,1)} fusion(bf16[256,2048]{1,0:T(8,128)(2,1)} %param.13, bf16[2048,1024]{1,0:T(8,128)(2,1)} %param.16), kind=kOutput, calls=%fused_computation.33 | convolution fusion | flops 1074003968 | bytes 5767168 | tf_op jit(solution)/shard_map/dot_general | solution.py:135
  43.6 2.2 reshape.310
  45.9 12.0 %all-to-all-done.1 = bf16[16,1,64,512]{3,2,1,0:T(8,128)(2,1)} async-done(((bf16[16,1,64,512]{3,2,1,0:T(8,128)(2,1)}), bf16[16,1,64,512]{3,2,1,0:T(8,128)(2,1)}, u32[]{:S(2)}, u32[]{:S(2)}) %all-to-all-start.1) | async-done | bytes 1048608 | tf_op jit(solution)/shard_map/all_to_all | solution.py:127
  67.3 6.0 %all-to-all-start.2 = ((bf16[16,1,64,512]{3,2,1,0:T(8,128)(2,1)}), bf16[16,1,64,512]{3,2,1,0:T(8,128)(2,1)}, u32[]{:S(2)}, u32[]{:S(2)}) async-start(bf16[16,1,64,512]{3,2,1,0:T(8,128)(2,1)} %bitcast.183), calls=%async_computation.3 | async-start | bytes 2097152 | tf_op jit(solution)/shard_map/all_to_all | solution.py:176
  73.5 2.6 convolution_convert_fusion.8
  76.1 20.2 %all-to-all-done.2 = bf16[16,1,64,512]{3,2,1,0:T(8,128)(2,1)} async-done(((bf16[16,1,64,512]{3,2,1,0:T(8,128)(2,1)}), bf16[16,1,64,512]{3,2,1,0:T(8,128)(2,1)}, u32[]{:S(2)}, u32[]{:S(2)}) %all-to-all-start.2) | async-done | bytes 1048608 | tf_op jit(solution)/shard_map/all_to_all | solution.py:176
  112.7 3.5 convolution_convert_fusion.4
  117.5 32.5 %collective-permute-done = f32[2048,256]{0,1:T(8,128)} collective-permute-done((f32[2048,256]{0,1:T(8,128)}, f32[2048,256]{0,1:T(8,128)}, u32[]{:S(2)}, u32[]{:S(2)}) %collective-permute-start) | collective-permute-done | bytes 2097184 | tf_op jit(solution)/shard_map/ppermute | solution.py:17
  149.9 2.7 add.111
  152.6 2.4 collective-permute-start.1
  160.6 37.2 %collective-permute-done.1 = f32[2048,256]{0,1:T(8,128)S(1)} collective-permute-done((f32[2048,256]{0,1:T(8,128)S(1)}, f32[2048,256]{0,1:T(8,128)S(1)}, u32[]{:S(2)}, u32[]{:S(2)}) %collective-permute-start.1) | collective-permute-done | bytes 2097184 | tf_op jit(solution)/shard_map/ppermute | solution.py:17
  199.5 4.4 %collective-permute-start.2 = (f32[2048,256]{0,1:T(8,128)}, f32[2048,256]{0,1:T(8,128)}, u32[]{:S(2)}, u32[]{:S(2)}) collective-permute-start(f32[2048,256]{0,1:T(8,128)} %add.112), channel_id=1, source_target_pairs={{0,8},{2,10},{4,12},{6,14},{8,0},{10,2},{12,4},{14,6},{16,24},{18,... | collective-permute-start | bytes 6291464 | tf_op jit(solution)/shard_map/ppermute | solution.py:17
  207.4 39.9 %collective-permute-done.2 = f32[2048,256]{0,1:T(8,128)} collective-permute-done((f32[2048,256]{0,1:T(8,128)}, f32[2048,256]{0,1:T(8,128)}, u32[]{:S(2)}, u32[]{:S(2)}) %collective-permute-start.2) | collective-permute-done | bytes 2097184 | tf_op jit(solution)/shard_map/ppermute | solution.py:17
  247.3 3.9 %add.113 = f32[2048,256]{0,1:T(8,128)} add(f32[2048,256]{0,1:T(8,128)} %add.112, f32[2048,256]{0,1:T(8,128)} %collective-permute-done.2) | non-fusion elementwise | flops 524288 | bytes 6291456 | tf_op jit(solution)/shard_map/add | solution.py:17
  251.1 2.9 collective-permute-start.3
  255.6 86.1 %collective-permute-done.3 = f32[2048,256]{0,1:T(8,128)} collective-permute-done((f32[2048,256]{0,1:T(8,128)}, f32[2048,256]{0,1:T(8,128)}, u32[]{:S(2)}, u32[]{:S(2)}) %collective-permute-start.3) | collective-permute-done | bytes 2097184 | tf_op jit(solution)/shard_map/ppermute | solution.py:17
  341.6 3.9 %add.114 = f32[2048,256]{0,1:T(8,128)} add(f32[2048,256]{0,1:T(8,128)} %add.113, f32[2048,256]{0,1:T(8,128)} %collective-permute-done.3) | non-fusion elementwise | flops 524288 | bytes 6291456 | tf_op jit(solution)/shard_map/add | solution.py:17
  345.5 2.9 copy.96
  (115 shorter events, 48.3 us)
Async XLA Ops:
  7.2 66.3 %copy-start = (bf16[2048,512]{1,0:T(8,128)(2,1)S(1)}, bf16[2048,512]{1,0:T(8,128)(2,1)}, u32[]{:S(2)}) copy-start(bf16[2048,512]{1,0:T(8,128)(2,1)} %param.19) | copy-start | bytes 6291460
  7.2 12.5 %copy-start.1 = (bf16[4,64,2048]{2,1,0:T(8,128)(2,1)S(1)}, bf16[4,64,2048]{2,1,0:T(8,128)(2,1)}, u32[]{:S(2)}) copy-start(bf16[4,64,2048]{2,1,0:T(8,128)(2,1)} %param.14) | copy-start | bytes 3145732
  9.1 15.6 %all-to-all-start = ((s32[16,1,1]{2,1,0:T(1,128)}), s32[16,1,1]{2,1,0:T(1,128)S(1)}, u32[]{:S(2)}, u32[]{:S(2)}) async-start(s32[16,1,1]{2,1,0:T(1,128)} %copy.79), calls=%async_computation | async-start | bytes 16384 | tf_op jit(solution)/shard_map/all_to_all | solution.py:110
  17.5 2.2 copy-start.7
  29.7 28.1 %all-to-all-start.1 = ((bf16[16,1,64,512]{3,2,1,0:T(8,128)(2,1)}), bf16[16,1,64,512]{3,2,1,0:T(8,128)(2,1)}, u32[]{:S(2)}, u32[]{:S(2)}) async-start(bf16[16,1,64,512]{3,2,1,0:T(8,128)(2,1)} %fusion.18), calls=%async_computation.1 | async-start | bytes 2097152 | tf_op jit(solution)/shard_map/all_to_all | solution.py:127
  34.1 5.0 %copy-start.16 = (f32[1024]{0:T(1024)S(1)}, f32[1024]{0:T(1024)}, u32[]{:S(2)}) copy-start(f32[1024]{0:T(1024)} %param.24) | copy-start | bytes 12292
  67.3 29.0 %all-to-all-start.2 = ((bf16[16,1,64,512]{3,2,1,0:T(8,128)(2,1)}), bf16[16,1,64,512]{3,2,1,0:T(8,128)(2,1)}, u32[]{:S(2)}, u32[]{:S(2)}) async-start(bf16[16,1,64,512]{3,2,1,0:T(8,128)(2,1)} %bitcast.183), calls=%async_computation.3 | async-start | bytes 2097152 | tf_op jit(solution)/shard_map/all_to_all | solution.py:176
  73.2 275.2 %reduce-scatter.3.cloned.1.call-start = ((), (), s32[]{:S(2)}) async-start(), calls=%async_computation.5 | async-start | bytes 1572864 | tf_op jit(solution)/shard_map/reduce_scatter | solution.py:212
  102.9 2.5 copy-start.11
  102.9 2.6 copy-start.20
  104.7 3.5 copy-start.22
  104.7 3.5 copy-start.17
  104.7 45.3 %collective-permute-start = (f32[2048,256]{0,1:T(8,128)}, f32[2048,256]{0,1:T(8,128)}, u32[]{:S(2)}, u32[]{:S(2)}) collective-permute-start(f32[2048,256]{0,1:T(8,128)} %fusion.1), channel_id=1, source_target_pairs={{0,2},{2,0},{4,6},{6,4},{8,10},{10,8},{12,14},{14,12},{16,18},{18,... | collective-permute-start | bytes 6291464 | tf_op jit(solution)/shard_map/ppermute | solution.py:17
  111.1 1.6 copy-start.21
  117.4 37.9 %copy-start.15 = (bf16[256,512]{0,1:T(8,128)(2,1)S(1)}, bf16[256,512]{0,1:T(8,128)(2,1)}, u32[]{:S(2)}) copy-start(bf16[256,512]{0,1:T(8,128)(2,1)} %copy.102) | copy-start | bytes 786436
  149.9 6.0 %copy-start.18 = (bf16[2048,1024]{1,0:T(8,128)(2,1)S(1)}, bf16[2048,1024]{1,0:T(8,128)(2,1)}, u32[]{:S(2)}) copy-start(bf16[2048,1024]{1,0:T(8,128)(2,1)} %param.21) | copy-start | bytes 12582916
  152.6 45.2 %collective-permute-start.1 = (f32[2048,256]{0,1:T(8,128)S(1)}, f32[2048,256]{0,1:T(8,128)S(1)}, u32[]{:S(2)}, u32[]{:S(2)}) collective-permute-start(f32[2048,256]{0,1:T(8,128)S(1)} %add.111), channel_id=1, source_target_pairs={{0,4},{2,6},{4,0},{6,2},{8,12},{10,14},{12,8},{14,10},{16,20},{18,... | collective-permute-start | bytes 6291464 | tf_op jit(solution)/shard_map/ppermute | solution.py:17
  156.0 2.5 copy-start.19
  160.6 43.2 %copy-start.12 = (bf16[2048,512]{1,0:T(8,128)(2,1)S(1)}, bf16[2048,512]{1,0:T(8,128)(2,1)}, u32[]{:S(2)}) copy-start(bf16[2048,512]{1,0:T(8,128)(2,1)} %param.20) | copy-start | bytes 6291460
  199.5 47.8 %collective-permute-start.2 = (f32[2048,256]{0,1:T(8,128)}, f32[2048,256]{0,1:T(8,128)}, u32[]{:S(2)}, u32[]{:S(2)}) collective-permute-start(f32[2048,256]{0,1:T(8,128)} %add.112), channel_id=1, source_target_pairs={{0,8},{2,10},{4,12},{6,14},{8,0},{10,2},{12,4},{14,6},{16,24},{18,... | collective-permute-start | bytes 6291464 | tf_op jit(solution)/shard_map/ppermute | solution.py:17
  203.8 1.8 copy-start.6
  205.6 142.8 %reduce-scatter.5.cloned.1.call-start = ((), (), s32[]{:S(2)}) async-start(), calls=%async_computation.6 | async-start | bytes 1572864 | tf_op jit(solution)/shard_map/reduce_scatter | solution.py:189
  207.4 46.7 %copy-start.8 = (bf16[2048,256]{1,0:T(8,128)(2,1)S(1)}, bf16[2048,256]{1,0:T(8,128)(2,1)}, u32[]{:S(2)}) copy-start(bf16[2048,256]{1,0:T(8,128)(2,1)} %param.18) | copy-start | bytes 3145732
  251.1 90.5 %collective-permute-start.3 = (f32[2048,256]{0,1:T(8,128)}, f32[2048,256]{0,1:T(8,128)}, u32[]{:S(2)}, u32[]{:S(2)}) collective-permute-start(f32[2048,256]{0,1:T(8,128)} %add.113), channel_id=1, source_target_pairs={{0,16},{2,18},{4,20},{6,22},{8,24},{10,26},{12,28},{14,30},{16,0},... | collective-permute-start | bytes 6291464 | tf_op jit(solution)/shard_map/ppermute | solution.py:17
  (8 other events, 9.7 us)
Sparse Core Ops, SparseCore 0:
  205.7 7.3 reduce-scatter.2
  255.7 6.3 reduce-scatter.4
